TPU v7x, 512 devices: a whole 4x8x8 slice. The times are simulated.
512 devices in a mesh: sp: 32 (over z, x), tp: 16 (over y, core).
Axes of the slice: x: 4, y: 8, z: 8, core: 2. Of those that a mesh axis runs over, the one named last changes fastest.
Arguments:
- residual: bfloat16 [8192, 2048], P('sp', 'tp'), may hold values from -26 to 26
- queries: bfloat16 [2048, 8192], P('tp', 'sp'), may hold values from -6 to 6
- keys: bfloat16 [2048, 8192], P('tp', 'sp'), may hold values from -6 to 6
- values: bfloat16 [2048, 8192], P('tp', 'sp'), may hold values from -12 to 12
- forget_cache: float32 [32, 8192], P('tp', 'sp'), as said below
- out_weight: bfloat16 [2048, 2048], P('tp'), may hold values from -0.125 to 0.125
- norm_gain: float32 [2048], replicated, may hold values from 0.1 to 1.9
- routes: int32 [8192, 2], P('sp'), may hold values from 0 to 31, all different within a row; in each aligned block of 256 rows (0 to 255, 256 to 511, ...) at most 20 rows name the same one
- route_weight: float32 [8192, 2], P('sp'), may hold values from 0.2 to 1
- gate_weight: bfloat16 [32, 2048, 4096], P('sp', None, 'tp'), may hold values from -0.125 to 0.125
- up_weight: bfloat16 [32, 2048, 4096], P('sp', None, 'tp'), may hold values from -0.125 to 0.125
- down_weight: bfloat16 [32, 4096, 2048], P('sp', 'tp'), may hold values from -0.09375 to 0.09375
Outputs:
- updated: bfloat16 [8192, 2048], P('sp', 'tp')
Inputs may be any that keep to these rules, and one draw needn't show every extreme that they name: `routes`: each row names 2 different experts; within the 256 rows of one index of sp no expert is named by more than 20 rows, and in the rows of some index some expert is named by exactly 20. `forget_cache`: each head's row never rises from one position to the next.
All inputs are finite; a program needn't handle non-finite values.
Results may differ from a plain program's by a relative error of at most 0.013.
Values may be sent and summed in bfloat16 or wider, within the bound.
No kernel may reach another device: no remote copies, remote signals or barrier semaphores. Data moves between devices by JAX's collectives and lax.ppermute only.
A program may use at most 64 MiB of HBM per device.

v0:
```python
import jax
import jax.numpy as jnp
from jax import lax
from jax.sharding import Mesh
from jax.sharding import PartitionSpec as P

SP = ("sp_0", "sp_1")
norm_eps = 1e-06
masked_score = -1e30
key_span = 1024


def gathered_by_axis(shard, axes, dim):
    out = shard
    for number in range(len(axes) - 1, -1, -1):
        out = lax.all_gather(out, axes[number], axis=dim, tiled=True)
    return out


def cut_along(shard, dim, peers):
    before, after = (shard.shape[:dim], shard.shape[dim + 1 :])
    return jnp.moveaxis(shard.reshape(*before, peers, -1, *after), dim, 0)


def sum_at_owner(shard, axis, dim):
    peers = lax.axis_size(axis)
    pieces = lax.all_to_all(cut_along(shard, dim, peers), axis, 0, 0, tiled=True)
    return jnp.sum(pieces.astype(jnp.float32), axis=0)


def sent_to_all(shard, axis):
    copies = jnp.broadcast_to(shard, (lax.axis_size(axis), *shard.shape))
    return lax.all_to_all(copies, axis, split_axis=0, concat_axis=0, tiled=True)


def taken_together(shard, axis):
    return sent_to_all(shard, axis).sum(axis=0)


def shards(
    residual,
    queries,
    keys,
    values,
    forget_cache,
    out_weight,
    norm_gain,
    routes,
    route_weight,
    gate_weight,
    up_weight,
    down_weight,
):
    sp_count = lax.axis_size(SP)
    token_count, local_width = residual.shape
    model_width = norm_gain.shape[0]
    head_count = forget_cache.shape[0]
    head_width = queries.shape[0] // head_count
    first_token = lax.axis_index(SP) * token_count
    last_token = first_token + token_count - 1
    query_heads = queries.reshape(head_count, head_width, token_count)
    query_place = first_token + jnp.arange(token_count, dtype=jnp.int32)
    score_scale = head_width ** (-0.5)

    def attend_block(state_now, key_block, value_block, cache_block, key_first):
        running_peak, running_total, running_sum = state_now
        block_length = key_block.shape[1]
        key_heads = key_block.reshape(head_count, head_width, block_length)
        value_heads = value_block.reshape(head_count, head_width, block_length)
        scores = (
            jnp.einsum("hdq,hdk->hqk", query_heads, key_heads, preferred_element_type=jnp.float32)
            * score_scale
        )
        scores = scores + forget_cache[:, :, None] - cache_block[:, None, :]
        key_place = key_first + jnp.arange(block_length, dtype=jnp.int32)
        allowed = key_place[None, :] <= query_place[:, None]
        scores = jnp.where(allowed[None], scores, masked_score)
        new_peak = jnp.maximum(running_peak, jnp.max(scores, axis=2))
        weights = jnp.exp(scores - new_peak[:, :, None])
        shrink = jnp.exp(running_peak - new_peak)
        new_total = running_total * shrink + jnp.sum(weights, axis=2)
        new_sum = running_sum * shrink[:, None, :] + jnp.einsum(
            "hdk,hqk->hdq",
            value_heads,
            weights.astype(jnp.bfloat16),
            preferred_element_type=jnp.float32,
        )
        return (new_peak, new_total, new_sum)

    initial = (
        jnp.full((head_count, token_count), masked_score, jnp.float32),
        jnp.zeros((head_count, token_count), jnp.float32),
        jnp.zeros((head_count, head_width, token_count), jnp.float32),
    )
    key_part = gathered_by_axis(keys.astype(jnp.float32), SP, 1).astype(jnp.bfloat16)
    value_part = gathered_by_axis(values.astype(jnp.float32), SP, 1).astype(jnp.bfloat16)
    cache_part = gathered_by_axis(forget_cache, SP, 1)
    part_length = key_part.shape[1]
    block_length = key_span

    def one_block(block_index, state_in):
        start_column = block_index * block_length
        key_block = lax.dynamic_slice_in_dim(key_part, start_column, block_length, 1)
        value_block = lax.dynamic_slice_in_dim(value_part, start_column, block_length, 1)
        cache_block = lax.dynamic_slice_in_dim(cache_part, start_column, block_length, 1)
        return lax.cond(
            start_column <= last_token,
            lambda inner: attend_block(inner, key_block, value_block, cache_block, start_column),
            lambda inner: inner,
            state_in,
        )

    final_peak, final_total, final_sum = lax.fori_loop(
        0, part_length // block_length, one_block, initial
    )
    attended = (
        (final_sum / final_total[:, None, :])
        .astype(jnp.bfloat16)
        .reshape(head_count * head_width, token_count)
    )
    projected = lax.dot_general(
        attended, out_weight, (((0,), (0,)), ((), ())), preferred_element_type=jnp.float32
    )
    head_sum = sum_at_owner(projected.astype(jnp.bfloat16), "tp", 1)
    stream = (residual.astype(jnp.float32) + head_sum).astype(jnp.bfloat16)
    top_count = routes.shape[1]
    item_count = token_count * top_count
    capacity = max(2, token_count * top_count * 5 // (4 * sp_count))
    expert_of = routes.reshape(item_count)
    onehot = (expert_of[:, None] == jnp.arange(sp_count, dtype=jnp.int32)[None, :]).astype(
        jnp.int32
    )
    earlier = jnp.cumsum(onehot, axis=0) - onehot
    target = expert_of * capacity + jnp.sum(earlier * onehot, axis=1)
    matches = target[None, :] == jnp.arange(sp_count * capacity, dtype=jnp.int32)[:, None]
    filled = jnp.any(matches, axis=1)
    source_row = (
        jnp.sum(jnp.where(matches, jnp.arange(item_count, dtype=jnp.int32)[None, :], 0), axis=1)
        // top_count
    )
    local_rows = stream.astype(jnp.float32)
    squares = taken_together(jnp.sum(local_rows * local_rows, axis=1), "tp")
    row_scale = lax.rsqrt(squares / model_width + norm_eps)
    local_gain = lax.dynamic_slice_in_dim(
        norm_gain, lax.axis_index("tp") * local_width, local_width
    )
    normed = (local_rows * row_scale[:, None] * local_gain[None, :]).astype(jnp.bfloat16)
    taken_rows = jnp.take(normed, source_row, axis=0)
    taken_rows = jnp.where(filled[:, None], taken_rows, jnp.zeros((), normed.dtype))
    arrived = lax.all_gather(
        lax.all_to_all(
            taken_rows.reshape(sp_count, capacity, normed.shape[1]),
            SP,
            split_axis=0,
            concat_axis=0,
            tiled=True,
        ),
        "tp",
        axis=2,
        tiled=True,
    )
    source_count = arrived.shape[0]
    slot_count = arrived.shape[1]
    flat_rows = arrived.reshape(source_count * slot_count, model_width)
    gate_value = jnp.dot(flat_rows, gate_weight[0], preferred_element_type=jnp.float32)
    up_value = jnp.dot(flat_rows, up_weight[0], preferred_element_type=jnp.float32)
    hidden = (jax.nn.silu(gate_value) * up_value).astype(jnp.bfloat16)
    down_value = jnp.dot(hidden, down_weight[0], preferred_element_type=jnp.float32)
    summed = sum_at_owner(
        down_value.reshape(source_count, slot_count, model_width).astype(jnp.bfloat16), "tp", 2
    )
    expert_back = lax.all_to_all(
        summed.astype(jnp.bfloat16), SP, split_axis=0, concat_axis=0, tiled=True
    )
    back_rows = expert_back.reshape(sp_count * capacity, local_width)
    picked = (
        jnp.take(back_rows, target, axis=0).astype(jnp.float32)
        * route_weight.reshape(item_count)[:, None]
    )
    mixture = jnp.sum(picked.reshape(token_count, top_count, local_width), axis=1)
    return (stream.astype(jnp.float32) + mixture).astype(jnp.bfloat16)


def solution(mesh):
    finer = Mesh(mesh.devices.reshape(8, 4, mesh.shape["tp"]), ("sp_0", "sp_1", "tp"))
    in_specs = (
        P(SP, "tp"),
        P("tp", SP),
        P("tp", SP),
        P("tp", SP),
        P("tp", SP),
        P("tp", None),
        P(),
        P(SP, None),
        P(SP, None),
        P(SP, None, "tp"),
        P(SP, None, "tp"),
        P(SP, "tp", None),
    )
    out_specs = P(SP, "tp")
    return jax.shard_map(
        shards, mesh=finer, in_specs=in_specs, out_specs=out_specs, check_vma=False
    )
```

profile of v0, /device:TPU:24, one launch (start us, length us, event | category | flops | bytes accessed | tf_op | source)
XLA Modules:
  0.0 361.6 jit_solution(1007863958048043251)
XLA Ops:
  6.5 14.3 %all_gather.21 = bf16[128,1024]{1,0:T(8,128)(2,1)} all-gather(bf16[128,256]{1,0:T(8,128)(2,1)} %param.18), channel_id=1, replica_groups=mesh['sp_0'=8,'sp_1'=4,'tp'=16] {'sp_1'}, dimensions={1}, use_global_device_ids=true | all-gather | bytes 327680 | tf_op jit(solution)/shard_map/all_gather | solution.py:16
  20.9 0.0 all-gather.4.cloned.1.call-update
  20.9 0.0 all-gather.6.cloned.1.call-start
  20.9 13.2 %all_gather.25 = bf16[128,1024]{1,0:T(8,128)(2,1)} all-gather(bf16[128,256]{1,0:T(8,128)(2,1)} %param.19), channel_id=1, replica_groups=mesh['sp_0'=8,'sp_1'=4,'tp'=16] {'sp_1'}, dimensions={1}, use_global_device_ids=true | all-gather | bytes 327680 | tf_op jit(solution)/shard_map/all_gather | solution.py:16
  34.1 0.0 all-gather.6.cloned.1.call-update
  34.2 10.6 %all_gather.23 = f32[2,1024]{1,0:T(2,128)S(1)} all-gather(f32[2,256]{1,0:T(2,128)} %param.20), channel_id=1, replica_groups=mesh['sp_0'=8,'sp_1'=4,'tp'=16] {'sp_1'}, dimensions={1}, use_global_device_ids=true | all-gather | bytes 10240 | tf_op jit(solution)/shard_map/all_gather | solution.py:16
  44.8 31.0 %all_gather.24 = f32[2,8192]{1,0:T(2,128)S(1)} all-gather(f32[2,1024]{1,0:T(2,128)S(1)} %all_gather.23), channel_id=1, replica_groups=mesh['sp_0'=8,'sp_1'=4,'tp'=16] {'sp_0'}, dimensions={1}, use_global_device_ids=true | all-gather | bytes 73728 | tf_op jit(solution)/shard_map/all_gather | solution.py:16
  75.7 36.7 %all-gather.6.cloned.1.call-done = bf16[128,8192]{1,0:T(8,128)(2,1)} async-done(((bf16[128,1024]{1,0:T(8,128)(2,1)}), bf16[128,8192]{1,0:T(8,128)(2,1)}) %all-gather.6.cloned.1.call-update) | async-done | bytes 2097168 | tf_op jit(solution)/shard_map/all_gather | solution.py:16
  112.5 4.2 %while.18 = (s32[]{:T(128)}, f32[2,256]{1,0:T(2,128)S(1)}, f32[2,256]{1,0:T(2,128)S(1)}, f32[2,64,256]{2,1,0:T(8,128)S(1)}, s32[]{:T(128)}, /*index=5*/bf16[128,...) while((s32[]{:T(128)}, f32[2,256]{1,0:T(2,128)S(1)}, ...), condition=%wide.region_5.6_spmd.clone, body=%wide.region_0.5_spmd.clone.sunk | while | flops 139266304 | bytes 8788313 | solution.py:113
  112.5 3.8 %conditional.3 = ((f32[2,256]{1,0:T(2,128)S(1)}, f32[2,256]{1,0:T(2,128)S(1)}, f32[2,64,256]{2,1,0:T(8,128)S(1)})) conditional(s32[]{:T(128)} %convert_element_type.119, (f32[2,256]{1,0:T(2,128)S(1)}, f32[2,256]{1,0:T(2,128)S(1)}, f32[2,64,256]{2,1,0:T(8,128)S(1)}) %tuple.55, (s32[]{:T(128)}, s32[]{:T(128)}, bf16[128,8192]{1,0:T(8,128)(2,1)}, ...), branch_computations={%region_1.0_spmd, %region_2.4_spmd} | conditional | flops 139266304 | bytes 8787026 | solution.py:106
  112.5 1.1 constant_dynamic-slice_fusion
  113.7 0.2 broadcast_compare_fusion
  113.9 1.6 fusion.26
  115.5 0.3 fusion.3
  115.8 0.5 convolution_add_fusion
  116.7 0.5 fusion.7
  117.2 1.3 copy.95
  118.4 7.4 %all-to-all-start = ((bf16[16,256,128]{2,1,0:T(8,128)(2,1)}), bf16[16,256,128]{2,1,0:T(8,128)(2,1)S(1)}, u32[]{:S(2)}, u32[]{:S(2)}) async-start(bf16[16,256,128]{2,1,0:T(8,128)(2,1)} %bitcast.60), calls=%async_computation | async-start | bytes 2097152 | tf_op jit(solution)/shard_map/all_to_all | solution.py:27
  125.8 0.1 copy.71
  126.0 0.1 eq.39
  126.1 0.1 reshape.233
  126.3 1.2 reduce-window.6
  127.4 0.2 slice_reduce_fusion
  127.7 0.1 fusion.21
  127.8 0.2 select_reduce_fusion
  128.0 0.1 reduce_sum.90
  128.2 0.2 fusion.8
  128.4 23.6 %all-to-all-done = bf16[16,256,128]{2,1,0:T(8,128)(2,1)S(1)} async-done(((bf16[16,256,128]{2,1,0:T(8,128)(2,1)}), bf16[16,256,128]{2,1,0:T(8,128)(2,1)S(1)}, u32[]{:S(2)}, u32[]{:S(2)}) %all-to-all-start) | async-done | bytes 1048608 | tf_op jit(solution)/shard_map/all_to_all | solution.py:27
  152.0 0.1 convert_reduce_fusion
  152.2 0.1 fusion.15
  152.3 0.6 broadcast_in_dim.101
  152.9 5.2 %all-to-all-start.1 = ((f32[16,1,256]{2,1,0:T(1,128)}), f32[16,1,256]{2,1,0:T(1,128)S(1)}, u32[]{:S(2)}, u32[]{:S(2)}) async-start(f32[16,1,256]{2,1,0:T(1,128)} %broadcast_in_dim.101), calls=%async_computation.1 | async-start | bytes 32768 | tf_op jit(solution)/shard_map/all_to_all | solution.py:33
  158.1 0.0 all-gather.8.cloned.1.call-start
  158.2 0.1 broadcast_in_dim.96
  158.3 0.8 dynamic_slice.42
  159.1 3.6 all-to-all-done.1
  162.7 0.1 fusion.17
  162.8 2.0 gather_fusion
  164.8 0.3 select_select_fusion
  165.1 44.1 %all_to_all.26 = bf16[32,20,128]{2,1,0:T(8,128)(2,1)} all-to-all(bf16[32,20,128]{2,1,0:T(8,128)(2,1)S(1)} %select_select_fusion), channel_id=1, replica_groups=mesh['sp_0'=8,'sp_1'=4,'tp'=16] {'sp_0','sp_1'}, dimensions={0} | all-to-all | bytes 327680 | tf_op jit(solution)/shard_map/all_to_all | solution.py:151
  209.2 0.0 all-gather.8.cloned.1.call-update
  209.2 39.2 %all-gather.8.cloned.1.call-done = bf16[32,20,2048]{2,1,0:T(8,128)(2,1)} async-done(((bf16[32,20,128]{2,1,0:T(8,128)(2,1)}), bf16[32,20,2048]{2,1,0:T(8,128)(2,1)}) %all-gather.8.cloned.1.call-update) | async-done | bytes 2621456 | tf_op jit(solution)/shard_map/all_gather | solution.py:150
  248.5 5.2 %reshape.235 = bf16[640,2048]{1,0:T(8,128)(2,1)} reshape(bf16[32,20,2048]{2,1,0:T(8,128)(2,1)} %all-gather.8.cloned.1.call-done) | data formatting | bytes 5242880 | tf_op jit(solution)/shard_map/reshape | solution.py:164
  253.7 2.7 fusion.12
  256.4 0.0 copy-done.7
  256.5 0.8 fusion.9
  257.3 0.1 dot_general.24
  257.4 0.9 fusion.6
  258.3 2.2 copy.94
  260.5 6.4 %all-to-all-start.3 = ((bf16[16,32,20,128]{3,1,2,0:T(8,128)(2,1)}), bf16[16,32,20,128]{3,1,2,0:T(8,128)(2,1)}, u32[]{:S(2)}, u32[]{:S(2)}) async-start(bf16[16,32,20,128]{3,1,2,0:T(8,128)(2,1)} %bitcast.62), calls=%async_computation.3 | async-start | bytes 5242880 | tf_op jit(solution)/shard_map/all_to_all | solution.py:27
  266.9 0.1 reduce_sum.88
  267.1 0.1 copy.81
  267.2 0.1 mul.123
  267.3 0.1 copy.74
  267.4 0.2 copy.75
  267.6 0.1 copy.82
  267.8 59.1 %all-to-all-done.3 = bf16[16,32,20,128]{3,1,2,0:T(8,128)(2,1)} async-done(((bf16[16,32,20,128]{3,1,2,0:T(8,128)(2,1)}), bf16[16,32,20,128]{3,1,2,0:T(8,128)(2,1)}, u32[]{:S(2)}, u32[]{:S(2)}) %all-to-all-start.3) | async-done | bytes 2621472 | tf_op jit(solution)/shard_map/all_to_all | solution.py:27
  326.9 2.1 reduce_sum.94
  329.0 0.7 copy.80
  329.8 9.9 %all-to-all-start.4 = ((bf16[32,20,128]{2,1,0:T(8,128)(2,1)}), bf16[32,20,128]{2,1,0:T(8,128)(2,1)S(1)}, u32[]{:S(2)}, u32[]{:S(2)}) async-start(bf16[32,20,128]{2,1,0:T(8,128)(2,1)} %copy.80), calls=%async_computation.4 | async-start | bytes 393216 | tf_op jit(solution)/shard_map/all_to_all | solution.py:172
  339.7 11.8 %all-to-all-done.4 = bf16[32,20,128]{2,1,0:T(8,128)(2,1)S(1)} async-done(((bf16[32,20,128]{2,1,0:T(8,128)(2,1)}), bf16[32,20,128]{2,1,0:T(8,128)(2,1)S(1)}, u32[]{:S(2)}, u32[]{:S(2)}) %all-to-all-start.4) | async-done | bytes 163872 | tf_op jit(solution)/shard_map/all_to_all | solution.py:172
  351.6 1.3 gather_fusion.1
  353.0 1.5 multiply_reduce_fusion
  354.4 0.7 fusion.18
  (57 shorter events, 0.5 us)
Async XLA Ops:
  6.5 250.9 %copy-start = (bf16[1,256,2048]{2,1,0:T(8,128)(2,1)S(1)}, bf16[1,256,2048]{2,1,0:T(8,128)(2,1)}, u32[]{:S(2)}) copy-start(bf16[1,256,2048]{2,1,0:T(8,128)(2,1)} %param.27) | copy-start | bytes 3145732
  6.5 69.2 %all-gather.4.cloned.1.call-start = ((), (), s32[]{:S(2)}) async-start(), calls=%async_computation.5 | async-start | bytes 2359296 | tf_op jit(solution)/shard_map/all_gather | solution.py:16
  20.9 91.5 %all-gather.6.cloned.1.call-start = ((), (), s32[]{:S(2)}) async-start(), calls=%async_computation.6 | async-start | bytes 2359296 | tf_op jit(solution)/shard_map/all_gather | solution.py:16
  112.4 4.2 %copy-start.2 = (bf16[128,2048]{1,0:T(8,128)(2,1)S(1)}, bf16[128,2048]{1,0:T(8,128)(2,1)}, u32[]{:S(2)}) copy-start(bf16[128,2048]{1,0:T(8,128)(2,1)} %param.21) | copy-start | bytes 1572868
  117.2 8.7 %copy-start.4 = (s32[256,2]{0,1:T(2,128)S(1)}, s32[256,2]{0,1:T(2,128)}, u32[]{:S(2)}) copy-start(s32[256,2]{0,1:T(2,128)} %param.23) | copy-start | bytes 6148
  118.4 33.7 %copy-start.3 = (bf16[256,128]{1,0:T(8,128)(2,1)S(1)}, bf16[256,128]{1,0:T(8,128)(2,1)}, u32[]{:S(2)}) copy-start(bf16[256,128]{1,0:T(8,128)(2,1)} %param.16) | copy-start | bytes 196612
  118.4 33.6 %all-to-all-start = ((bf16[16,256,128]{2,1,0:T(8,128)(2,1)}), bf16[16,256,128]{2,1,0:T(8,128)(2,1)S(1)}, u32[]{:S(2)}, u32[]{:S(2)}) async-start(bf16[16,256,128]{2,1,0:T(8,128)(2,1)} %bitcast.60), calls=%async_computation | async-start | bytes 2097152 | tf_op jit(solution)/shard_map/all_to_all | solution.py:27
  152.9 9.7 %all-to-all-start.1 = ((f32[16,1,256]{2,1,0:T(1,128)}), f32[16,1,256]{2,1,0:T(1,128)S(1)}, u32[]{:S(2)}, u32[]{:S(2)}) async-start(f32[16,1,256]{2,1,0:T(1,128)} %broadcast_in_dim.101), calls=%async_computation.1 | async-start | bytes 32768 | tf_op jit(solution)/shard_map/all_to_all | solution.py:33
  158.1 90.4 %all-gather.8.cloned.1.call-start = ((), (), s32[]{:S(2)}) async-start(), calls=%async_computation.7 | async-start | bytes 3342336 | tf_op jit(solution)/shard_map/all_gather | solution.py:150
  209.2 44.4 %copy-start.6 = (bf16[1,2048,256]{2,1,0:T(8,128)(2,1)S(1)}, bf16[1,2048,256]{2,1,0:T(8,128)(2,1)}, u32[]{:S(2)}) copy-start(bf16[1,2048,256]{2,1,0:T(8,128)(2,1)} %param.25) | copy-start | bytes 3145732
  253.7 2.8 copy-start.1
  253.7 2.8 copy-start.7
  260.5 7.2 %copy-start.5 = (f32[256,2]{0,1:T(2,128)S(1)}, f32[256,2]{0,1:T(2,128)}, u32[]{:S(2)}) copy-start(f32[256,2]{0,1:T(2,128)} %param.24) | copy-start | bytes 6148
  260.5 66.5 %all-to-all-start.3 = ((bf16[16,32,20,128]{3,1,2,0:T(8,128)(2,1)}), bf16[16,32,20,128]{3,1,2,0:T(8,128)(2,1)}, u32[]{:S(2)}, u32[]{:S(2)}) async-start(bf16[16,32,20,128]{3,1,2,0:T(8,128)(2,1)} %bitcast.62), calls=%async_computation.3 | async-start | bytes 5242880 | tf_op jit(solution)/shard_map/all_to_all | solution.py:27
  329.8 21.8 %all-to-all-start.4 = ((bf16[32,20,128]{2,1,0:T(8,128)(2,1)}), bf16[32,20,128]{2,1,0:T(8,128)(2,1)S(1)}, u32[]{:S(2)}, u32[]{:S(2)}) async-start(bf16[32,20,128]{2,1,0:T(8,128)(2,1)} %copy.80), calls=%async_computation.4 | async-start | bytes 393216 | tf_op jit(solution)/shard_map/all_to_all | solution.py:172
Sparse Core Ops, SparseCore 0:
  21.0 47.3 all-gather.3
  70.5 41.8 all-gather.5
  209.3 39.0 all-gather.7
where the time goes:
time: 363 us; the launch traced here: 362 us
  waiting for transfers between devices  174 us (48%)
  blocking collectives  113 us (31%)
  starting transfers between devices  29 us (8%)
  local copies, waits for them, and re-layouts  17.1 us (5%)
  between operations  13.4 us (4%)
  other arithmetic  7.3 us (2%)
  matrix products  6.94 us (2%)
    all_to_all x2, waiting for transfers between devices, sum_at_owner(): lax.all_to_all(cut_along(shard, dim, peers), axis, 0, 0, tiled=True)  82.8 us
    all_gather x4, blocking collectives, gathered_by_axis(): out = lax.all_gather(out, axes[number], axis=dim, tiled=True)  69.1 us
    all_to_all x1, blocking collectives, shards(): lax.all_to_all(taken_rows.reshape(sp_count, capacity, normed.shape[1]), S...  44.1 us
    all_gather x1, waiting for transfers between devices, shards(): lax.all_gather(lax.all_to_all(taken_rows.reshape(sp_count, capacity, norm...  39.2 us
    all_gather x2, waiting for transfers between devices, gathered_by_axis(): out = lax.all_gather(out, axes[number], axis=dim, tiled=True)  36.7 us
    all_to_all x2, starting transfers between devices, sum_at_owner(): lax.all_to_all(cut_along(shard, dim, peers), axis, 0, 0, tiled=True)  13.8 us
    all_to_all x1, waiting for transfers between devices, shards(): lax.all_to_all(summed.astype(jnp.bfloat16), SP, split_axis=0, concat_axis...  11.8 us
    all_to_all x1, starting transfers between devices, shards(): lax.all_to_all(summed.astype(jnp.bfloat16), SP, split_axis=0, concat_axis...  9.92 us
  transfers between devices with their start and end apart: 7, of which 6 were waited for; matrix products, arithmetic and copies ran while one was open for 1% of the time, Pallas kernels for 0%

commit v1 on v0

--- a/solution.py
+++ b/solution.py
@@ -147,18 +147,15 @@
     normed = (local_rows * row_scale[:, None] * local_gain[None, :]).astype(jnp.bfloat16)
     taken_rows = jnp.take(normed, source_row, axis=0)
     taken_rows = jnp.where(filled[:, None], taken_rows, jnp.zeros((), normed.dtype))
-    arrived = lax.all_gather(
-        lax.all_to_all(
-            taken_rows.reshape(sp_count, capacity, normed.shape[1]),
-            SP,
-            split_axis=0,
-            concat_axis=0,
-            tiled=True,
-        ),
-        "tp",
-        axis=2,
+    block = lax.all_to_all(
+        taken_rows.reshape(sp_count, capacity, normed.shape[1]),
+        SP,
+        split_axis=0,
+        concat_axis=0,
         tiled=True,
     )
+    sent = jnp.stack([block] * lax.axis_size("tp"))
+    arrived = jnp.concatenate(lax.all_to_all(sent, "tp", 0, 0), axis=2)
     source_count = arrived.shape[0]
     slot_count = arrived.shape[1]
     flat_rows = arrived.reshape(source_count * slot_count, model_width)

time: 363 us -> 379 us (1.044)
  blocking collectives: 113 us -> 179 us
  waiting for transfers between devices: 174 us -> 135 us
  starting transfers between devices: 29 us -> 22.1 us
    all_to_all x0 -> x1, blocking collectives: none -> 65.6 us  [shards(): arrived = jnp.concatenate(lax.all_to_all(sent, 'tp', 0, 0), axis=2)]
    all_gather x1 -> x0, waiting for transfers between devices: 39.2 us -> none  [shards(): lax.all_gather(lax.all_to_all(taken_rows.reshape(sp_count, capacity, norm...]
    all_to_all x1, starting transfers between devices: 9.92 us -> 3.87 us  [shards(): lax.all_to_all(summed.astype(jnp.bfloat16), SP, split_axis=0, concat_axis...]
  transfers between devices with their start and end apart: 7 -> 6, of which waited for: 6 -> 5; matrix products, arithmetic and copies ran while one was open for 1% -> 1% of each run, Pallas kernels for 0% -> 0%
where the time goes in v1:
time: 379 us; the launch traced here: 377 us
  blocking collectives  179 us (47%)
  waiting for transfers between devices  135 us (36%)
  starting transfers between devices  22.1 us (6%)
  local copies, waits for them, and re-layouts  14.5 us (4%)
  between operations  13.7 us (4%)
  other arithmetic  7.3 us (2%)
  matrix products  5.04 us (1%)
    all_to_all x2, waiting for transfers between devices, sum_at_owner(): lax.all_to_all(cut_along(shard, dim, peers), axis, 0, 0, tiled=True)  82.8 us
    all_gather x4, blocking collectives, gathered_by_axis(): out = lax.all_gather(out, axes[number], axis=dim, tiled=True)  69.1 us
    all_to_all x1, blocking collectives, shards(): arrived = jnp.concatenate(lax.all_to_all(sent, 'tp', 0, 0), axis=2)  65.6 us
    all_to_all x1, blocking collectives, shards(): lax.all_to_all(taken_rows.reshape(sp_count, capacity, normed.shape[1]), S...  44 us
    all_gather x2, waiting for transfers between devices, gathered_by_axis(): out = lax.all_gather(out, axes[number], axis=dim, tiled=True)  36.7 us
    all_to_all x2, starting transfers between devices, sum_at_owner(): lax.all_to_all(cut_along(shard, dim, peers), axis, 0, 0, tiled=True)  13 us
    all_to_all x1, waiting for transfers between devices, shards(): lax.all_to_all(summed.astype(jnp.bfloat16), SP, split_axis=0, concat_axis...  12.3 us
  transfers between devices with their start and end apart: 6, of which 5 were waited for; matrix products, arithmetic and copies ran while one was open for 1% of the time, Pallas kernels for 0%

profile of v1, /device:TPU:24, one launch (start us, length us, event | category | flops | bytes accessed | tf_op | source)
XLA Modules:
  0.0 377.3 jit_solution(3463351888011368954)
XLA Ops:
  6.5 14.3 %all_gather.18 = bf16[128,1024]{1,0:T(8,128)(2,1)} all-gather(bf16[128,256]{1,0:T(8,128)(2,1)} %param.18), channel_id=1, replica_groups=mesh['sp_0'=8,'sp_1'=4,'tp'=16] {'sp_1'}, dimensions={1}, use_global_device_ids=true | all-gather | bytes 327680 | tf_op jit(solution)/shard_map/all_gather | solution.py:16
  20.9 0.0 all-gather.3.cloned.1.call-update
  20.9 0.0 all-gather.5.cloned.1.call-start
  20.9 13.2 %all_gather.22 = bf16[128,1024]{1,0:T(8,128)(2,1)} all-gather(bf16[128,256]{1,0:T(8,128)(2,1)} %param.19), channel_id=1, replica_groups=mesh['sp_0'=8,'sp_1'=4,'tp'=16] {'sp_1'}, dimensions={1}, use_global_device_ids=true | all-gather | bytes 327680 | tf_op jit(solution)/shard_map/all_gather | solution.py:16
  34.1 0.0 all-gather.5.cloned.1.call-update
  34.2 10.6 %all_gather.20 = f32[2,1024]{1,0:T(2,128)S(1)} all-gather(f32[2,256]{1,0:T(2,128)} %param.20), channel_id=1, replica_groups=mesh['sp_0'=8,'sp_1'=4,'tp'=16] {'sp_1'}, dimensions={1}, use_global_device_ids=true | all-gather | bytes 10240 | tf_op jit(solution)/shard_map/all_gather | solution.py:16
  44.8 31.0 %all_gather.21 = f32[2,8192]{1,0:T(2,128)S(1)} all-gather(f32[2,1024]{1,0:T(2,128)S(1)} %all_gather.20), channel_id=1, replica_groups=mesh['sp_0'=8,'sp_1'=4,'tp'=16] {'sp_0'}, dimensions={1}, use_global_device_ids=true | all-gather | bytes 73728 | tf_op jit(solution)/shard_map/all_gather | solution.py:16
  75.7 36.7 %all-gather.5.cloned.1.call-done = bf16[128,8192]{1,0:T(8,128)(2,1)} async-done(((bf16[128,1024]{1,0:T(8,128)(2,1)}), bf16[128,8192]{1,0:T(8,128)(2,1)}) %all-gather.5.cloned.1.call-update) | async-done | bytes 2097168 | tf_op jit(solution)/shard_map/all_gather | solution.py:16
  112.4 0.0 copy-start.1
  112.5 4.2 %while.18 = (s32[]{:T(128)}, f32[2,256]{1,0:T(2,128)S(1)}, f32[2,256]{1,0:T(2,128)S(1)}, f32[2,64,256]{2,1,0:T(8,128)S(1)}, s32[]{:T(128)}, /*index=5*/bf16[128,...) while((s32[]{:T(128)}, f32[2,256]{1,0:T(2,128)S(1)}, ...), condition=%wide.region_5.6_spmd.clone, body=%wide.region_0.5_spmd.clone.sunk | while | flops 139266304 | bytes 8788313 | solution.py:113
  112.5 3.8 %conditional.3 = ((f32[2,256]{1,0:T(2,128)S(1)}, f32[2,256]{1,0:T(2,128)S(1)}, f32[2,64,256]{2,1,0:T(8,128)S(1)})) conditional(s32[]{:T(128)} %convert_element_type.119, (f32[2,256]{1,0:T(2,128)S(1)}, f32[2,256]{1,0:T(2,128)S(1)}, f32[2,64,256]{2,1,0:T(8,128)S(1)}) %tuple.55, (s32[]{:T(128)}, s32[]{:T(128)}, bf16[128,8192]{1,0:T(8,128)(2,1)}, ...), branch_computations={%region_1.0_spmd, %region_2.4_spmd} | conditional | flops 139266304 | bytes 8787026 | solution.py:106
  112.5 1.1 constant_dynamic-slice_fusion
  113.7 0.2 broadcast_compare_fusion
  113.9 1.6 fusion.36
  115.5 0.3 fusion.3
  115.8 0.5 convolution_add_fusion
  116.7 0.5 fusion.13
  117.2 1.3 copy.117
  118.4 7.4 %all-to-all-start = ((bf16[16,256,128]{2,1,0:T(8,128)(2,1)}), bf16[16,256,128]{2,1,0:T(8,128)(2,1)S(1)}, u32[]{:S(2)}, u32[]{:S(2)}) async-start(bf16[16,256,128]{2,1,0:T(8,128)(2,1)} %bitcast.70), calls=%async_computation | async-start | bytes 2097152 | tf_op jit(solution)/shard_map/all_to_all | solution.py:27
  125.8 0.1 copy.78
  126.0 0.1 eq.39
  126.1 0.1 reshape.235
  126.3 1.2 reduce-window.6
  127.5 0.2 slice_reduce_fusion
  127.7 0.1 fusion.31
  127.8 0.2 select_reduce_fusion
  128.0 0.1 reduce_sum.90
  128.2 0.2 fusion.14
  128.4 23.6 %all-to-all-done = bf16[16,256,128]{2,1,0:T(8,128)(2,1)S(1)} async-done(((bf16[16,256,128]{2,1,0:T(8,128)(2,1)}), bf16[16,256,128]{2,1,0:T(8,128)(2,1)S(1)}, u32[]{:S(2)}, u32[]{:S(2)}) %all-to-all-start) | async-done | bytes 1048608 | tf_op jit(solution)/shard_map/all_to_all | solution.py:27
  152.0 0.1 convert_reduce_fusion
  152.2 0.1 fusion.25
  152.3 0.6 broadcast_in_dim.101
  152.9 5.2 %all-to-all-start.1 = ((f32[16,1,256]{2,1,0:T(1,128)}), f32[16,1,256]{2,1,0:T(1,128)S(1)}, u32[]{:S(2)}, u32[]{:S(2)}) async-start(f32[16,1,256]{2,1,0:T(1,128)} %broadcast_in_dim.101), calls=%async_computation.1 | async-start | bytes 32768 | tf_op jit(solution)/shard_map/all_to_all | solution.py:33
  158.2 0.1 broadcast_in_dim.96
  158.3 0.8 dynamic_slice.42
  159.0 3.6 all-to-all-done.1
  162.7 0.1 fusion.27
  162.8 2.0 gather_fusion
  164.9 0.3 select_select_fusion
  165.1 44.0 %all_to_all.31 = bf16[32,20,128]{2,1,0:T(8,128)(2,1)S(1)} all-to-all(bf16[32,20,128]{2,1,0:T(8,128)(2,1)S(1)} %select_select_fusion), channel_id=1, replica_groups=mesh['sp_0'=8,'sp_1'=4,'tp'=16] {'sp_0','sp_1'}, dimensions={0} | all-to-all | bytes 327680 | tf_op jit(solution)/shard_map/all_to_all | solution.py:150
  209.1 0.5 stack.2
  209.6 65.6 %all_to_all.32 = bf16[16,32,20,128]{3,1,2,0:T(8,128)(2,1)S(1)} all-to-all(bf16[16,32,20,128]{3,1,2,0:T(8,128)(2,1)S(1)} %stack.2), channel_id=1, replica_groups=mesh['sp_0'=8,'sp_1'=4,'tp'=16] {'tp'}, dimensions={0} | all-to-all | bytes 5242880 | tf_op jit(solution)/shard_map/all_to_all | solution.py:158
  275.3 1.7 copy.85
  277.0 0.8 fusion.8
  277.8 0.4 copy-done.6
  278.2 0.9 fusion.18
  279.1 0.1 dot_general.24
  279.1 0.8 fusion.12
  280.0 2.2 copy.116
  282.2 5.6 %all-to-all-start.4 = ((bf16[16,32,20,128]{3,1,2,0:T(8,128)(2,1)}), bf16[16,32,20,128]{3,1,2,0:T(8,128)(2,1)}, u32[]{:S(2)}, u32[]{:S(2)}) async-start(bf16[16,32,20,128]{3,1,2,0:T(8,128)(2,1)} %bitcast.72), calls=%async_computation.4 | async-start | bytes 5242880 | tf_op jit(solution)/shard_map/all_to_all | solution.py:27
  287.8 0.1 reduce_sum.88
  288.0 0.1 copy.90
  288.1 0.1 mul.123
  288.3 0.1 copy.81
  288.4 0.2 copy.82
  288.6 0.1 copy.91
  288.7 59.1 %all-to-all-done.4 = bf16[16,32,20,128]{3,1,2,0:T(8,128)(2,1)} async-done(((bf16[16,32,20,128]{3,1,2,0:T(8,128)(2,1)}), bf16[16,32,20,128]{3,1,2,0:T(8,128)(2,1)}, u32[]{:S(2)}, u32[]{:S(2)}) %all-to-all-start.4) | async-done | bytes 2621472 | tf_op jit(solution)/shard_map/all_to_all | solution.py:27
  347.9 2.1 reduce_sum.94
  350.0 0.7 copy.89
  350.7 3.9 %all-to-all-start.5 = ((bf16[32,20,128]{2,1,0:T(8,128)(2,1)}), bf16[32,20,128]{2,1,0:T(8,128)(2,1)S(1)}, u32[]{:S(2)}, u32[]{:S(2)}) async-start(bf16[32,20,128]{2,1,0:T(8,128)(2,1)} %copy.89), calls=%async_computation.5 | async-start | bytes 393216 | tf_op jit(solution)/shard_map/all_to_all | solution.py:169
  354.6 12.3 %all-to-all-done.5 = bf16[32,20,128]{2,1,0:T(8,128)(2,1)S(1)} async-done(((bf16[32,20,128]{2,1,0:T(8,128)(2,1)}), bf16[32,20,128]{2,1,0:T(8,128)(2,1)S(1)}, u32[]{:S(2)}, u32[]{:S(2)}) %all-to-all-start.5) | async-done | bytes 163872 | tf_op jit(solution)/shard_map/all_to_all | solution.py:169
  367.0 1.3 gather_fusion.1
  368.3 1.5 multiply_reduce_fusion
  369.8 0.7 fusion.28
  (55 shorter events, 0.5 us)
Async XLA Ops:
  6.5 272.6 %copy-start = (bf16[1,256,2048]{2,1,0:T(8,128)(2,1)S(1)}, bf16[1,256,2048]{2,1,0:T(8,128)(2,1)}, u32[]{:S(2)}) copy-start(bf16[1,256,2048]{2,1,0:T(8,128)(2,1)} %param.27) | copy-start | bytes 3145732
  6.5 69.2 %all-gather.3.cloned.1.call-start = ((), (), s32[]{:S(2)}) async-start(), calls=%async_computation.6 | async-start | bytes 2359296 | tf_op jit(solution)/shard_map/all_gather | solution.py:16
  20.9 91.5 %all-gather.5.cloned.1.call-start = ((), (), s32[]{:S(2)}) async-start(), calls=%async_computation.7 | async-start | bytes 2359296 | tf_op jit(solution)/shard_map/all_gather | solution.py:16
  112.4 4.2 %copy-start.1 = (bf16[128,2048]{1,0:T(8,128)(2,1)S(1)}, bf16[128,2048]{1,0:T(8,128)(2,1)}, u32[]{:S(2)}) copy-start(bf16[128,2048]{1,0:T(8,128)(2,1)} %param.21) | copy-start | bytes 1572868
  117.2 8.7 %copy-start.3 = (s32[256,2]{0,1:T(2,128)S(1)}, s32[256,2]{0,1:T(2,128)}, u32[]{:S(2)}) copy-start(s32[256,2]{0,1:T(2,128)} %param.23) | copy-start | bytes 6148
  118.4 33.8 %copy-start.2 = (bf16[256,128]{1,0:T(8,128)(2,1)S(1)}, bf16[256,128]{1,0:T(8,128)(2,1)}, u32[]{:S(2)}) copy-start(bf16[256,128]{1,0:T(8,128)(2,1)} %param.16) | copy-start | bytes 196612
  118.4 33.6 %all-to-all-start = ((bf16[16,256,128]{2,1,0:T(8,128)(2,1)}), bf16[16,256,128]{2,1,0:T(8,128)(2,1)S(1)}, u32[]{:S(2)}, u32[]{:S(2)}) async-start(bf16[16,256,128]{2,1,0:T(8,128)(2,1)} %bitcast.70), calls=%async_computation | async-start | bytes 2097152 | tf_op jit(solution)/shard_map/all_to_all | solution.py:27
  152.9 9.7 %all-to-all-start.1 = ((f32[16,1,256]{2,1,0:T(1,128)}), f32[16,1,256]{2,1,0:T(1,128)S(1)}, u32[]{:S(2)}, u32[]{:S(2)}) async-start(f32[16,1,256]{2,1,0:T(1,128)} %broadcast_in_dim.101), calls=%async_computation.1 | async-start | bytes 32768 | tf_op jit(solution)/shard_map/all_to_all | solution.py:33
  275.3 1.7 copy-start.5
  277.0 1.2 copy-start.6
  282.2 6.4 %copy-start.4 = (f32[256,2]{0,1:T(2,128)S(1)}, f32[256,2]{0,1:T(2,128)}, u32[]{:S(2)}) copy-start(f32[256,2]{0,1:T(2,128)} %param.24) | copy-start | bytes 6148
  282.2 65.7 %all-to-all-start.4 = ((bf16[16,32,20,128]{3,1,2,0:T(8,128)(2,1)}), bf16[16,32,20,128]{3,1,2,0:T(8,128)(2,1)}, u32[]{:S(2)}, u32[]{:S(2)}) async-start(bf16[16,32,20,128]{3,1,2,0:T(8,128)(2,1)} %bitcast.72), calls=%async_computation.4 | async-start | bytes 5242880 | tf_op jit(solution)/shard_map/all_to_all | solution.py:27
  350.7 16.2 %all-to-all-start.5 = ((bf16[32,20,128]{2,1,0:T(8,128)(2,1)}), bf16[32,20,128]{2,1,0:T(8,128)(2,1)S(1)}, u32[]{:S(2)}, u32[]{:S(2)}) async-start(bf16[32,20,128]{2,1,0:T(8,128)(2,1)} %copy.89), calls=%async_computation.5 | async-start | bytes 393216 | tf_op jit(solution)/shard_map/all_to_all | solution.py:169
Sparse Core Ops, SparseCore 0:
  21.0 47.3 all-gather.2
  70.5 41.8 all-gather.4
